TPU v7x, 32 devices: a whole 2x2x4 slice. The times are simulated.
32 devices in a mesh: ep: 16 (over z, y, x), tp: 2 (over core).
Axes of the slice: x: 2, y: 2, z: 4, core: 2. Of those that a mesh axis runs over, the one named last changes fastest.
Arguments:
- tokens: bfloat16 [512, 3072], P('ep'), may hold values from -6 to 6
- carried: float32 [512, 96, 128], P('ep', 'tp'), may hold values from -4 to 4
- decay_rate: float32 [96, 64], P('tp'), may hold values from 0.02 to 20
- frequency: float32 [96, 64], P('tp'), may hold values from 0 to 200
- log_step: float32 [96], P('tp'), may hold values from -4.6 to 0
- in_map: bfloat16 [96, 128, 16], P('tp'), may hold values from -1 to 1
- out_map: bfloat16 [96, 16, 128], P('tp'), may hold values from -0.5 to 0.5
- skip_gain: float32 [1536], P('tp'), may hold values from -4 to 4
- norm_gain: float32 [3072], replicated, may hold values from 0.1 to 1.9
- w_in: bfloat16 [3072, 1536], P(None, 'tp'), may hold values from -0.109375 to 0.109375
- w_out: bfloat16 [1536, 3072], P('tp'), may hold values from -0.15625 to 0.15625
- expert_gain: float32 [3072], replicated, may hold values from 0.1 to 1.9
- route_ids: int32 [512, 2], P('ep'), may hold values from 0 to 7, all different within a row; in each aligned block of 32 rows (0 to 31, 32 to 63, ...) at most 16 rows name the same one
- route_logit: float32 [512, 2], P('ep'), may hold values from -6 to 6
- w_gate: bfloat16 [3072, 43008], P(None, ('ep', 'tp')), may hold values from -0.109375 to 0.109375
- w_up: bfloat16 [3072, 43008], P(None, ('ep', 'tp')), may hold values from -0.109375 to 0.109375
- w_down: bfloat16 [43008, 3072], P(('ep', 'tp')), may hold values from -0.078125 to 0.078125
Outputs:
- new_tokens: bfloat16 [512, 3072], P('ep', 'tp')
- new_carried: float32 [512, 96, 128], P('ep', 'tp')
Inputs may be any that keep to these rules, and one draw needn't show every extreme that they name: `route_ids`: each row names 2 different experts; within each aligned block of 32 rows (the rows of one index of ep) no expert is named by more than 16 rows, a bound that some block reaches.
All inputs are finite; a program needn't handle non-finite values.
Results may differ from a plain program's by a relative error of at most 0.014.
Values may be sent and summed in bfloat16 or wider, within the bound.
A program may use at most 128 MiB of HBM per device.

v0:
```python
import jax
import jax.numpy as jnp
from jax import lax
from jax.sharding import PartitionSpec as P

EXPERTS = 8
TOP = 2
CAP = 16


def normalize(rows, gain):
    wide = rows.astype(jnp.float32)
    scaled = wide * lax.rsqrt(jnp.mean(wide * wide, axis=-1, keepdims=True) + 1e-06)
    return (scaled * gain).astype(jnp.bfloat16)


def state_update(drive, carried, decay_rate, frequency, log_step, in_map, out_map, skip_gain):
    count_rows, width = drive.shape
    groups, half = decay_rate.shape
    channels = width // groups
    step_size = jnp.exp(log_step)[:, None]
    magnitude = jnp.exp(-decay_rate * step_size)
    real_decay = magnitude * jnp.cos(frequency * step_size)
    imag_decay = magnitude * jnp.sin(frequency * step_size)
    denom = decay_rate * decay_rate + frequency * frequency
    real_less = real_decay - 1.0
    real_factor = (-real_less * decay_rate + imag_decay * frequency) / denom
    imag_factor = (-imag_decay * decay_rate - real_less * frequency) / denom
    grouped_drive = drive.reshape(count_rows, groups, channels)
    projected = jnp.einsum(
        "sgh,gqh->sgq", grouped_drive, in_map, preferred_element_type=jnp.float32
    )
    real_in = projected[..., :half]
    imag_in = projected[..., half:]
    real_push = real_factor * real_in - imag_factor * imag_in
    imag_push = real_factor * imag_in + imag_factor * real_in
    real_old = carried[..., :half]
    imag_old = carried[..., half:]
    real_new = real_decay * real_old - imag_decay * imag_old + real_push
    imag_new = real_decay * imag_old + imag_decay * real_old + imag_push
    joined = jnp.concatenate([real_new, -imag_new], axis=-1)
    reading = jnp.einsum(
        "sgq,ghq->sgh", joined, out_map.astype(jnp.float32), precision=lax.Precision.HIGHEST
    )
    total = reading.reshape(count_rows, width) + skip_gain * drive.astype(jnp.float32)
    activated = jax.nn.gelu(total).astype(jnp.bfloat16)
    return (activated, jnp.concatenate([real_new, imag_new], axis=-1))


def route_weights(route_logit):
    first = jax.nn.sigmoid(route_logit[:, 0] - route_logit[:, 1])
    second = jax.nn.sigmoid(route_logit[:, 1] - route_logit[:, 0])
    return jnp.stack([first, second], axis=1)


def per_device(
    tokens,
    carried,
    decay_rate,
    frequency,
    log_step,
    in_map,
    out_map,
    skip_gain,
    norm_gain,
    w_in,
    w_out,
    expert_gain,
    route_ids,
    route_logit,
    w_gate,
    w_up,
    w_down,
):
    count_rows, model_width = tokens.shape
    normed = normalize(tokens, norm_gain)
    drive = jnp.dot(normed, w_in, preferred_element_type=jnp.float32).astype(jnp.bfloat16)
    activated, new_carried = state_update(
        drive, carried, decay_rate, frequency, log_step, in_map, out_map, skip_gain
    )
    partial_value = jnp.dot(activated, w_out, preferred_element_type=jnp.float32).astype(
        jnp.bfloat16
    )
    summed = lax.psum(partial_value.astype(jnp.float32).astype(jnp.bfloat16), "tp").astype(
        jnp.float32
    )
    mixed = (tokens.astype(jnp.float32) + summed).astype(jnp.bfloat16)
    expert_in = normalize(mixed, expert_gain)
    weights = route_weights(route_logit)
    ep_count = lax.axis_size("ep")
    group_size = ep_count // EXPERTS
    expert_ids = jnp.arange(EXPERTS, dtype=jnp.int32)
    routes_flat = route_ids.reshape(-1)
    weights_flat = weights.reshape(-1)
    onehot = (routes_flat[:, None] == expert_ids[None, :]).astype(jnp.int32)
    earlier = jnp.cumsum(onehot, axis=0) - onehot
    slot_index = jnp.sum(earlier * onehot, axis=1)
    position = routes_flat * CAP + slot_index
    placement = (jnp.arange(EXPERTS * CAP, dtype=jnp.int32)[:, None] == position[None, :]).astype(
        jnp.float32
    )
    per_token = placement.reshape(EXPERTS * CAP, count_rows, TOP).sum(axis=2)
    packed = jnp.dot(per_token.astype(jnp.bfloat16), expert_in, preferred_element_type=jnp.float32)
    packed = packed.astype(jnp.bfloat16).reshape(EXPERTS, CAP, model_width)
    outgoing = jnp.repeat(packed, group_size, axis=0)
    received = lax.all_to_all(outgoing, "ep", split_axis=0, concat_axis=0, tiled=True)
    sources, slots, features = received.shape
    rows = received.reshape(sources * slots, features)
    gated = jnp.dot(rows, w_gate, preferred_element_type=jnp.float32)
    upward = jnp.dot(rows, w_up, preferred_element_type=jnp.float32)
    hidden = (jax.nn.silu(gated) * upward).astype(jnp.bfloat16)
    produced = jnp.dot(hidden, w_down, preferred_element_type=jnp.float32)
    produced = produced.reshape(sources, slots, features)
    halves = lax.psum_scatter(
        produced.astype(jnp.bfloat16), "tp", scatter_dimension=2, tiled=True
    ).astype(jnp.float32)
    returned = lax.all_to_all(
        halves.astype(jnp.bfloat16), "ep", split_axis=0, concat_axis=0, tiled=True
    ).astype(halves.dtype)
    per_expert = returned.reshape(EXPERTS, group_size, CAP, -1).sum(axis=1)
    per_expert = per_expert.reshape(EXPERTS * CAP, -1)
    weighing = (
        (placement * weights_flat[None, :]).reshape(EXPERTS * CAP, count_rows, TOP).sum(axis=2)
    )
    expert_sum = jnp.dot(
        weighing.T, per_expert, preferred_element_type=jnp.float32, precision=lax.Precision.HIGHEST
    )
    half_width = model_width // lax.axis_size("tp")
    column_start = lax.axis_index("tp") * half_width
    own_mixed = lax.dynamic_slice_in_dim(mixed, column_start, half_width, 1)
    new_tokens = (own_mixed.astype(jnp.float32) + expert_sum).astype(jnp.bfloat16)
    return (new_tokens, new_carried)


def solution(mesh):
    return jax.shard_map(
        per_device,
        mesh=mesh,
        in_specs=(
            P("ep", None),
            P("ep", "tp", None),
            P("tp", None),
            P("tp", None),
            P("tp"),
            P("tp", None, None),
            P("tp", None, None),
            P("tp"),
            P(),
            P(None, "tp"),
            P("tp", None),
            P(),
            P("ep", None),
            P("ep", None),
            P(None, ("ep", "tp")),
            P(None, ("ep", "tp")),
            P(("ep", "tp"), None),
        ),
        out_specs=(P("ep", "tp"), P("ep", "tp", None)),
        check_vma=False,
    )
```

profile of v0, /device:TPU:0, one launch (start us, length us, event | category | flops | bytes accessed | tf_op | source)
XLA Modules:
  0.0 152.5 jit_solution(15072366406423989595)
XLA Ops:
  7.2 0.7 exp.18
  7.9 1.1 fusion.9
  9.0 3.5 %convolution_convert_fusion.3 = bf16[32,768]{1,0:T(8,128)(2,1)S(1)} fusion(bf16[3072,768]{1,0:T(8,128)(2,1)} %param.26, bf16[32,3072]{1,0:T(8,128)(2,1)} %param.17, f32[3072]{0:T(1024)} %param.25, f32[32]{0:T(128)S(1)} %add_rsqrt_fusion.1), kind=kOutput, calls=%fused_computation.9 | convolution fusion | flops 151412736 | bytes 4976768 | tf_op jit(solution)/shard_map/dot_general | solution.py:77
  12.5 0.2 copy.48
  12.7 0.3 fusion.44
  13.0 0.3 convolution_bitcast_fusion
  13.4 0.2 cosine_multiply_fusion
  13.6 0.8 fusion.43
  14.6 0.8 fusion.2
  15.6 4.0 %convolution_convert_fusion.2 = bf16[32,3072]{1,0:T(8,128)(2,1)} fusion(bf16[768,3072]{1,0:T(8,128)(2,1)} %param.27, f32[32,768]{1,0:T(8,128)S(1)} %copy.49, bf16[32,768]{1,0:T(8,128)(2,1)S(1)} %convolution_convert_fusion.3, f32[768]{0:T(1024)S(1)} %copy-done.8), kind=kOutput, calls=%fused_computation.2 | convolution fusion | flops 151388160 | bytes 5065728 | tf_op jit(solution)/shard_map/dot_general | solution.py:81
  20.0 0.2 select_reduce_fusion.1
  20.5 20.0 %all-reduce.2.cloned.1.call-done = bf16[32,3072]{1,0:T(8,128)(2,1)} async-done(((bf16[32,3072]{1,0:T(8,128)(2,1)}), bf16[32,3072]{1,0:T(8,128)(2,1)}) %all-reduce.2.cloned.1.call-update) | async-done | bytes 196624 | tf_op jit(solution)/shard_map/psum | solution.py:84
  40.5 1.1 fusion.6
  41.6 0.4 convolution_convert_fusion.1
  42.1 0.2 broadcast_in_dim.2
  42.3 44.6 %all_to_all.10 = bf16[16,16,3072]{2,1,0:T(8,128)(2,1)S(1)} all-to-all(bf16[16,16,3072]{2,1,0:T(8,128)(2,1)S(1)} %bitcast.27), channel_id=1, replica_groups=mesh['ep'=16,'tp'=2] {'ep'}, dimensions={0} | all-to-all | bytes 3145728 | tf_op jit(solution)/shard_map/all_to_all | solution.py:106
  86.9 6.8 %fusion.45 = f32[256,1344]{0,1:T(8,128)} fusion(bf16[256,3072]{1,0:T(8,128)(2,1)S(1)} %bitcast.31, bf16[3072,1344]{0,1:T(8,128)(2,1)} %param.31), kind=kOutput, calls=%fused_computation.74 | convolution fusion | flops 2113929216 | bytes 11206656 | tf_op jit(solution)/shard_map/dot_general | solution.py:109
  93.6 16.3 %convolution_convert_fusion = bf16[256,3072]{1,0:T(8,128)(2,1)} fusion(bf16[1344,3072]{1,0:T(8,128)(2,1)} %param.33, bf16[256,3072]{1,0:T(8,128)(2,1)S(1)} %bitcast.32, bf16[3072,1344]{0,1:T(8,128)(2,1)} %param.32, f32[256,1344]{0,1:T(8,128)} %fusion.45), kind=kOutput, calls=%fused_computation | convolution fusion | flops 4230709248 | bytes 21037056 | tf_op jit(solution)/shard_map/dot_general | solution.py:112
  110.0 7.5 %reduce-scatter.2.cloned.1.call-done = bf16[16,16,1536]{2,1,0:T(8,128)(2,1)} async-done(((bf16[16,16,3072]{2,1,0:T(8,128)(2,1)}), bf16[16,16,1536]{2,1,0:T(8,128)(2,1)}) %reduce-scatter.2.cloned.1.call-update) | async-done | bytes 786448 | tf_op jit(solution)/shard_map/reduce_scatter | solution.py:114
  117.4 6.9 %all-to-all-start.1 = ((bf16[16,16,1536]{2,1,0:T(8,128)(2,1)}), bf16[16,16,1536]{2,1,0:T(8,128)(2,1)S(1)}, u32[]{:S(2)}, u32[]{:S(2)}) async-start(bf16[16,16,1536]{2,1,0:T(8,128)(2,1)} %reduce-scatter.2.cloned.1.call-done), calls=%async_computation.2 | async-start | bytes 1572864 | tf_op jit(solution)/shard_map/all_to_all | solution.py:117
  124.3 0.3 pad_maximum_fusion
  124.6 1.3 copy.52
  126.0 18.4 %all-to-all-done.1 = bf16[16,16,1536]{2,1,0:T(8,128)(2,1)S(1)} async-done(((bf16[16,16,1536]{2,1,0:T(8,128)(2,1)}), bf16[16,16,1536]{2,1,0:T(8,128)(2,1)S(1)}, u32[]{:S(2)}, u32[]{:S(2)}) %all-to-all-start.1) | async-done | bytes 786464 | tf_op jit(solution)/shard_map/all_to_all | solution.py:117
  144.5 1.2 fusion.1
  (38 shorter events, 1.4 us)
Async XLA Ops:
  7.2 5.8 %copy-start = (bf16[48,128,16]{1,2,0:T(8,128)(2,1)S(1)}, bf16[48,128,16]{1,2,0:T(8,128)(2,1)}, u32[]{:S(2)}) copy-start(bf16[48,128,16]{1,2,0:T(8,128)(2,1)} %param.22) | copy-start | bytes 589828
  7.2 33.3 %all-reduce.2.cloned.1.call-start = ((), (), s32[]{:S(2)}) async-start(), calls=%async_computation.3 | async-start | bytes 393216 | tf_op jit(solution)/shard_map/psum | solution.py:84
  9.0 3.7 %copy-start.1 = (f32[32,48,128]{2,1,0:T(8,128)S(1)}, f32[32,48,128]{2,1,0:T(8,128)}, u32[]{:S(2)}) copy-start(f32[32,48,128]{2,1,0:T(8,128)} %param.18) | copy-start | bytes 2359300
  12.7 0.7 copy-start.4
  12.7 0.7 copy-start.5
  13.6 0.9 copy-start.3
  14.4 1.1 copy-start.8
  15.5 4.1 %copy-start.9 = (f32[32,2]{0,1:T(2,128)S(1)}, f32[32,2]{0,1:T(2,128)}, u32[]{:S(2)}) copy-start(f32[32,2]{0,1:T(2,128)} %param.30) | copy-start | bytes 772
  15.6 4.1 %copy-start.7 = (s32[32,2]{0,1:T(2,128)S(1)}, s32[32,2]{0,1:T(2,128)}, u32[]{:S(2)}) copy-start(s32[32,2]{0,1:T(2,128)} %param.29) | copy-start | bytes 772
  15.6 25.0 %copy-start.2 = (bf16[32,3072]{1,0:T(8,128)(2,1)S(1)}, bf16[32,3072]{1,0:T(8,128)(2,1)}, u32[]{:S(2)}) copy-start(bf16[32,3072]{1,0:T(8,128)(2,1)} %param.17) | copy-start | bytes 589828
  15.6 26.1 %copy-start.6 = (f32[3072]{0:T(1024)S(1)}, f32[3072]{0:T(1024)}, u32[]{:S(2)}) copy-start(f32[3072]{0:T(1024)} %param.28) | copy-start | bytes 36868
  19.6 97.9 %reduce-scatter.2.cloned.1.call-start = ((), (), s32[]{:S(2)}) async-start(), calls=%async_computation.4 | async-start | bytes 2359296 | tf_op jit(solution)/shard_map/reduce_scatter | solution.py:114
  117.4 26.9 %all-to-all-start.1 = ((bf16[16,16,1536]{2,1,0:T(8,128)(2,1)}), bf16[16,16,1536]{2,1,0:T(8,128)(2,1)S(1)}, u32[]{:S(2)}, u32[]{:S(2)}) async-start(bf16[16,16,1536]{2,1,0:T(8,128)(2,1)} %reduce-scatter.2.cloned.1.call-done), calls=%async_computation.2 | async-start | bytes 1572864 | tf_op jit(solution)/shard_map/all_to_all | solution.py:117
Sparse Core Ops, SparseCore 0:
  19.7 20.7 all-reduce.1
  110.1 7.2 reduce-scatter.1
where the time goes:
time: 153 us; the launch traced here: 152 us
  waiting for transfers between devices  45.9 us (30%)
  blocking collectives  44.6 us (29%)
  matrix products  33.3 us (22%)
  between operations  14.3 us (9%)
  starting transfers between devices  6.98 us (5%)
  other arithmetic  4.03 us (3%)
  local copies, waits for them, and re-layouts  3.47 us (2%)
    all_to_all x1, blocking collectives, per_device(): lax.all_to_all(outgoing, 'ep', split_axis=0, concat_axis=0, tiled=True)  44.6 us
    psum x1, waiting for transfers between devices, per_device(): lax.psum(partial_value.astype(jnp.float32).astype(jnp.bfloat16), 'tp')  20 us
    all_to_all x1, waiting for transfers between devices, per_device(): lax.all_to_all(halves.astype(jnp.bfloat16), 'ep', split_axis=0, concat_ax...  18.4 us
    dot_general x1, matrix products, per_device(): produced = jnp.dot(hidden, w_down, preferred_element_type=jnp.float32)  16.3 us
    reduce_scatter x1, waiting for transfers between devices, per_device(): lax.psum_scatter(produced.astype(jnp.bfloat16), 'tp', scatter_dimension=2...  7.46 us
    all_to_all x1, starting transfers between devices, per_device(): lax.all_to_all(halves.astype(jnp.bfloat16), 'ep', split_axis=0, concat_ax...  6.9 us
    dot_general x1, matrix products, per_device(): gated = jnp.dot(rows, w_gate, preferred_element_type=jnp.float32)  6.77 us
    dot_general x1, matrix products, per_device(): jnp.dot(activated, w_out, preferred_element_type=jnp.float32)  3.96 us
  transfers between devices with their start and end apart: 3, of which 3 were waited for; matrix products, arithmetic and copies ran while one was open for 2% of the time, Pallas kernels for 0%

commit v1 on v0

--- a/solution.py
+++ b/solution.py
@@ -1,6 +1,10 @@
+import functools
+
 import jax
 import jax.numpy as jnp
 from jax import lax
+from jax.experimental import pallas as pl
+from jax.experimental.pallas import tpu as pltpu
 from jax.sharding import PartitionSpec as P
 
 EXPERTS = 8
@@ -51,6 +55,376 @@
     first = jax.nn.sigmoid(route_logit[:, 0] - route_logit[:, 1])
     second = jax.nn.sigmoid(route_logit[:, 1] - route_logit[:, 0])
     return jnp.stack([first, second], axis=1)
+
+
+MESH = pl.DeviceIdType.MESH
+SEND_ORDER = (1, 2, 4, 6, 5, 7, 3)
+WAIT_ORDER = (0, 1, 2, 4, 6, 5, 7, 3)
+BACK_ORDER = (4, 6, 5, 7, 2, 3, 1)
+PIECES = 3
+BLOCK = 256
+
+
+def dot_transposed(rows, weights):
+    return lax.dot_general(
+        rows, weights, (((1,), (1,)), ((), ())), preferred_element_type=jnp.float32
+    )
+
+
+def expert_kernel(
+    group_size,
+    tokens,
+    activated,
+    gain,
+    pack,
+    weight_high,
+    weight_low,
+    mix_hbm,
+    gate_hbm,
+    up_hbm,
+    down_hbm,
+    out,
+    mix,
+    gate,
+    up,
+    down,
+    partial,
+    partial_in,
+    mixed_buf,
+    normed_buf,
+    packed,
+    rows_buf,
+    hidden,
+    swap_out,
+    swap_in,
+    own_sum,
+    peer_out,
+    peer_in,
+    back_out,
+    returned,
+    load_sem,
+    partial_sem,
+    direct_send,
+    direct_recv,
+    peer_send,
+    peer_recv,
+    core_send,
+    core_recv,
+    swap_send,
+    swap_recv,
+    sum_send,
+    sum_recv,
+    back_send,
+    back_recv,
+    local_sem,
+):
+    ep = lax.axis_index("ep")
+    core = lax.axis_index("tp")
+    expert = ep // group_size
+    lane = ep % group_size
+    other = 1 - core
+    model_width = tokens.shape[1]
+    half = model_width // 2
+    hidden_units = gate_hbm.shape[0]
+    sources = rows_buf.shape[1]
+    total_rows = sources * CAP
+    piece = half // PIECES
+
+    def at_expert(step):
+        place, bit = 0, 1
+        while bit < EXPERTS:
+            place = place + bit * lax.rem(expert // bit + step // bit, 2)
+            bit *= 2
+        return place
+
+    def at_lane(step):
+        return lax.rem(lane + step + group_size, group_size)
+
+    mix_parts = 4
+    mix_span = model_width // mix_parts
+    mix_loads = []
+    for part in range(mix_parts):
+        span = pl.ds(part * mix_span, mix_span)
+        mix_loads.append(
+            pltpu.make_async_copy(mix_hbm.at[:, span], mix.at[:, span], load_sem.at[5 + part])
+        )
+        mix_loads[-1].start()
+    loads = []
+    for part in range(2):
+        span = pl.ds(part * (hidden_units // 2), hidden_units // 2)
+        loads.append(pltpu.make_async_copy(gate_hbm.at[span], gate.at[span], load_sem.at[2 * part]))
+        loads.append(pltpu.make_async_copy(up_hbm.at[span], up.at[span], load_sem.at[2 * part + 1]))
+    loads.append(pltpu.make_async_copy(down_hbm, down, load_sem.at[4]))
+
+    barrier = pltpu.get_barrier_semaphore()
+    pl.semaphore_signal(barrier, inc=1, device_id=(ep, other), device_id_type=MESH)
+    for step in range(1, EXPERTS):
+        target = at_expert(step) * group_size + lane
+        pl.semaphore_signal(barrier, inc=1, device_id=(target, core), device_id_type=MESH)
+    for step in range(1, group_size):
+        target = expert * group_size + at_lane(step)
+        pl.semaphore_signal(barrier, inc=1, device_id=(target, core), device_id_type=MESH)
+    for part in range(mix_parts):
+        span = pl.ds(part * mix_span, mix_span)
+        mix_loads[part].wait()
+        if part == mix_parts - 2:
+            for load in loads:
+                load.start()
+        partial[:, span] = jnp.dot(
+            activated[...], mix[:, span], preferred_element_type=jnp.float32
+        ).astype(jnp.bfloat16)
+    pl.semaphore_wait(barrier, EXPERTS + group_size - 1)
+
+    def remote(source, target, send, recv, place):
+        return pltpu.make_async_remote_copy(
+            src_ref=source,
+            dst_ref=target,
+            send_sem=send,
+            recv_sem=recv,
+            device_id=place,
+            device_id_type=MESH,
+        )
+
+    exchange = remote(partial, partial_in, partial_sem.at[0], partial_sem.at[1], (ep, other))
+    exchange.start()
+    exchange.wait()
+
+    summed = partial[...].astype(jnp.float32) + partial_in[...].astype(jnp.float32)
+    mixed = (tokens[...].astype(jnp.float32) + summed).astype(jnp.bfloat16)
+    mixed_buf[...] = mixed
+    normed_buf[...] = normalize(mixed, gain[...])
+    own_columns = pl.ds(pl.multiple_of(core * half, 128), half)
+    chosen = jnp.dot(pack[...], normed_buf[:, own_columns], preferred_element_type=jnp.float32)
+    packed[...] = chosen.astype(jnp.bfloat16).reshape(EXPERTS, CAP, half)
+
+    def direct(step):
+        place = at_expert(step)
+        return remote(
+            packed.at[place],
+            rows_buf.at[core, ep],
+            direct_send.at[step],
+            direct_recv.at[step],
+            (place * group_size + lane, core),
+        )
+
+    def to_peer(step, shift):
+        source = at_expert(step) * group_size + lane
+        return remote(
+            rows_buf.at[core, source],
+            rows_buf.at[core, source],
+            peer_send.at[shift, step],
+            peer_recv.at[shift, step],
+            (expert * group_size + at_lane(shift), core),
+        )
+
+    def to_core(step, shift):
+        source = at_expert(step) * group_size + at_lane(-shift)
+        return remote(
+            rows_buf.at[core, source],
+            rows_buf.at[core, source],
+            core_send.at[shift, step],
+            core_recv.at[shift, step],
+            (ep, other),
+        )
+
+    def from_core(step, shift):
+        source = at_expert(step) * group_size + at_lane(-shift)
+        return remote(
+            rows_buf.at[other, source],
+            rows_buf.at[other, source],
+            core_send.at[shift, step],
+            core_recv.at[shift, step],
+            (ep, other),
+        )
+
+    for step in SEND_ORDER:
+        direct(step).start()
+    own_copy = pltpu.make_async_copy(packed.at[expert], rows_buf.at[core, ep], local_sem)
+    own_copy.start()
+    for step in WAIT_ORDER:
+        if step == 0:
+            own_copy.wait()
+        else:
+            direct(step).wait_recv()
+        for shift in range(1, group_size):
+            to_peer(step, shift).start()
+        to_core(step, 0).start()
+    for step in WAIT_ORDER:
+        for shift in range(1, group_size):
+            to_peer(step, shift).wait_recv()
+            to_core(step, shift).start()
+    for step in WAIT_ORDER:
+        for shift in range(group_size):
+            from_core(step, shift).wait_recv()
+    for load in loads[:4]:
+        load.wait()
+
+    def hidden_block(columns):
+        low = rows_buf[0].reshape(total_rows, half)
+        high = rows_buf[1].reshape(total_rows, half)
+
+        def project(weights):
+            return dot_transposed(low, weights[columns, :half]) + dot_transposed(
+                high, weights[columns, half:]
+            )
+
+        hidden[:, columns] = (jax.nn.silu(project(gate)) * project(up)).astype(jnp.bfloat16)
+
+    blocks = hidden_units // BLOCK
+
+    def hidden_step(index, carry):
+        hidden_block(pl.ds(pl.multiple_of(index * BLOCK, BLOCK), BLOCK))
+        return carry
+
+    lax.fori_loop(0, blocks, hidden_step, 0)
+    if hidden_units % BLOCK:
+        hidden_block(pl.ds(blocks * BLOCK, hidden_units % BLOCK))
+
+    loads[4].wait()
+
+    def produce(owner, index):
+        columns = pl.ds(pl.multiple_of(owner * half + index * piece, 128), piece)
+        return jnp.dot(hidden[...], down[:, columns], preferred_element_type=jnp.float32)
+
+    def swap(index):
+        return remote(
+            swap_out.at[index],
+            swap_in.at[index],
+            swap_send.at[index],
+            swap_recv.at[index],
+            (ep, other),
+        )
+
+    def sum_to_peer(index, shift):
+        place = at_lane(shift)
+        return remote(
+            peer_out.at[index, place],
+            peer_in.at[index, shift - 1],
+            sum_send.at[index, shift],
+            sum_recv.at[index, shift],
+            (expert * group_size + place, core),
+        )
+
+    def give_back(index, step):
+        place = at_expert(step)
+        return remote(
+            back_out.at[index, place],
+            returned.at[index, expert],
+            back_send.at[index, step],
+            back_recv.at[index, step],
+            (place * group_size + lane, core),
+        )
+
+    def start_swap(index):
+        swap_out[index] = produce(other, index).astype(jnp.bfloat16)
+        swap(index).start()
+
+    start_swap(0)
+    for index in range(PIECES):
+        if index + 1 < PIECES:
+            start_swap(index + 1)
+        value = produce(core, index)
+        swap(index).wait_recv()
+        value = value + swap_in[index].astype(jnp.float32)
+        value = value.reshape(EXPERTS, group_size, CAP, piece)
+        for place in range(group_size):
+            own_sum[index, place] = value[:, place]
+            peer_out[index, place] = value[:, place].astype(jnp.bfloat16)
+        for shift in range(1, group_size):
+            sum_to_peer(index, shift).start()
+    for index in range(PIECES):
+        value = own_sum[index, lane]
+        for shift in range(1, group_size):
+            sum_to_peer(index, shift).wait_recv()
+            value = value + peer_in[index, shift - 1].astype(jnp.float32)
+        back_out[index] = value.astype(jnp.bfloat16)
+        for step in BACK_ORDER:
+            give_back(index, step).start()
+        returned[index, expert] = back_out[index, expert]
+    for index in range(PIECES):
+        for step in range(1, EXPERTS):
+            give_back(index, step).wait_recv()
+        rows = returned[index].reshape(EXPERTS * CAP, piece)
+        value = jnp.dot(weight_high[...], rows, preferred_element_type=jnp.float32)
+        value = value + jnp.dot(weight_low[...], rows, preferred_element_type=jnp.float32)
+        columns = pl.ds(pl.multiple_of(core * half + index * piece, 128), piece)
+        value = value + mixed_buf[:, columns].astype(jnp.float32)
+        out[:, index * piece : (index + 1) * piece] = value.astype(out.dtype)
+
+    for step in range(1, EXPERTS):
+        direct(step).wait_send()
+    for step in range(EXPERTS):
+        for shift in range(group_size):
+            to_core(step, shift).wait_send()
+            if shift:
+                to_peer(step, shift).wait_send()
+    for index in range(PIECES):
+        swap(index).wait_send()
+        for shift in range(1, group_size):
+            sum_to_peer(index, shift).wait_send()
+        for step in range(1, EXPERTS):
+            give_back(index, step).wait_send()
+
+
+def experts(
+    tokens, activated, gain, pack, weight_high, weight_low, w_out, w_gate, w_up, w_down
+):
+    count_rows, model_width = tokens.shape
+    sources = lax.axis_size("ep")
+    group_size = sources // EXPERTS
+    half = model_width // 2
+    piece = half // PIECES
+    hidden_units = w_gate.shape[0]
+    total_rows = sources * CAP
+    peers = max(group_size - 1, 1)
+    dma = pltpu.SemaphoreType.DMA
+    narrow = jnp.bfloat16
+    vmem = pl.BlockSpec(memory_space=pltpu.VMEM)
+    anywhere = pl.BlockSpec(memory_space=pl.ANY)
+    return pl.pallas_call(
+        functools.partial(expert_kernel, group_size),
+        out_shape=jax.ShapeDtypeStruct((count_rows, half), narrow),
+        in_specs=[vmem] * 6 + [anywhere] * 4,
+        out_specs=vmem,
+        scratch_shapes=[
+            pltpu.VMEM(w_out.shape, narrow),
+            pltpu.VMEM(w_gate.shape, narrow),
+            pltpu.VMEM(w_up.shape, narrow),
+            pltpu.VMEM(w_down.shape, narrow),
+            pltpu.VMEM((count_rows, model_width), narrow),
+            pltpu.VMEM((count_rows, model_width), narrow),
+            pltpu.VMEM((count_rows, model_width), narrow),
+            pltpu.VMEM((count_rows, model_width), narrow),
+            pltpu.VMEM((EXPERTS, CAP, half), narrow),
+            pltpu.VMEM((2, sources, CAP, half), narrow),
+            pltpu.VMEM((total_rows, hidden_units), narrow),
+            pltpu.VMEM((PIECES, total_rows, piece), narrow),
+            pltpu.VMEM((PIECES, total_rows, piece), narrow),
+            pltpu.VMEM((PIECES, group_size, EXPERTS, CAP, piece), jnp.float32),
+            pltpu.VMEM((PIECES, group_size, EXPERTS, CAP, piece), narrow),
+            pltpu.VMEM((PIECES, peers, EXPERTS, CAP, piece), narrow),
+            pltpu.VMEM((PIECES, EXPERTS, CAP, piece), narrow),
+            pltpu.VMEM((PIECES, EXPERTS, CAP, piece), narrow),
+            dma((9,)),
+            dma((2,)),
+            dma((EXPERTS,)),
+            dma((EXPERTS,)),
+            dma((group_size, EXPERTS)),
+            dma((group_size, EXPERTS)),
+            dma((group_size, EXPERTS)),
+            dma((group_size, EXPERTS)),
+            dma((PIECES,)),
+            dma((PIECES,)),
+            dma((PIECES, group_size)),
+            dma((PIECES, group_size)),
+            dma((PIECES, EXPERTS)),
+            dma((PIECES, EXPERTS)),
+            dma,
+        ],
+        compiler_params=pltpu.CompilerParams(
+            collective_id=0, has_side_effects=True, vmem_limit_bytes=56 * 1024 * 1024
+        ),
+    )(tokens, activated, gain, pack, weight_high, weight_low, w_out, w_gate, w_up, w_down)
 
 
 def per_device(
@@ -78,17 +452,7 @@
     activated, new_carried = state_update(
         drive, carried, decay_rate, frequency, log_step, in_map, out_map, skip_gain
     )
-    partial_value = jnp.dot(activated, w_out, preferred_element_type=jnp.float32).astype(
-        jnp.bfloat16
-    )
-    summed = lax.psum(partial_value.astype(jnp.float32).astype(jnp.bfloat16), "tp").astype(
-        jnp.float32
-    )
-    mixed = (tokens.astype(jnp.float32) + summed).astype(jnp.bfloat16)
-    expert_in = normalize(mixed, expert_gain)
     weights = route_weights(route_logit)
-    ep_count = lax.axis_size("ep")
-    group_size = ep_count // EXPERTS
     expert_ids = jnp.arange(EXPERTS, dtype=jnp.int32)
     routes_flat = route_ids.reshape(-1)
     weights_flat = weights.reshape(-1)
@@ -99,36 +463,25 @@
     placement = (jnp.arange(EXPERTS * CAP, dtype=jnp.int32)[:, None] == position[None, :]).astype(
         jnp.float32
     )
-    per_token = placement.reshape(EXPERTS * CAP, count_rows, TOP).sum(axis=2)
-    packed = jnp.dot(per_token.astype(jnp.bfloat16), expert_in, preferred_element_type=jnp.float32)
-    packed = packed.astype(jnp.bfloat16).reshape(EXPERTS, CAP, model_width)
-    outgoing = jnp.repeat(packed, group_size, axis=0)
-    received = lax.all_to_all(outgoing, "ep", split_axis=0, concat_axis=0, tiled=True)
-    sources, slots, features = received.shape
-    rows = received.reshape(sources * slots, features)
-    gated = jnp.dot(rows, w_gate, preferred_element_type=jnp.float32)
-    upward = jnp.dot(rows, w_up, preferred_element_type=jnp.float32)
-    hidden = (jax.nn.silu(gated) * upward).astype(jnp.bfloat16)
-    produced = jnp.dot(hidden, w_down, preferred_element_type=jnp.float32)
-    produced = produced.reshape(sources, slots, features)
-    halves = lax.psum_scatter(
-        produced.astype(jnp.bfloat16), "tp", scatter_dimension=2, tiled=True
-    ).astype(jnp.float32)
-    returned = lax.all_to_all(
-        halves.astype(jnp.bfloat16), "ep", split_axis=0, concat_axis=0, tiled=True
-    ).astype(halves.dtype)
-    per_expert = returned.reshape(EXPERTS, group_size, CAP, -1).sum(axis=1)
-    per_expert = per_expert.reshape(EXPERTS * CAP, -1)
+    pack = placement.reshape(EXPERTS * CAP, count_rows, TOP).sum(axis=2).astype(jnp.bfloat16)
     weighing = (
         (placement * weights_flat[None, :]).reshape(EXPERTS * CAP, count_rows, TOP).sum(axis=2)
-    )
-    expert_sum = jnp.dot(
-        weighing.T, per_expert, preferred_element_type=jnp.float32, precision=lax.Precision.HIGHEST
-    )
-    half_width = model_width // lax.axis_size("tp")
-    column_start = lax.axis_index("tp") * half_width
-    own_mixed = lax.dynamic_slice_in_dim(mixed, column_start, half_width, 1)
-    new_tokens = (own_mixed.astype(jnp.float32) + expert_sum).astype(jnp.bfloat16)
+    ).T
+    weight_high = lax.reduce_precision(weighing, 8, 7)
+    weight_low = (weighing - weight_high).astype(jnp.bfloat16)
+    weight_high = weight_high.astype(jnp.bfloat16)
+    new_tokens = experts(
+        tokens,
+        activated,
+        expert_gain.reshape(1, model_width),
+        pack,
+        weight_high,
+        weight_low,
+        w_out,
+        w_gate.T,
+        w_up.T,
+        w_down,
+    )
     return (new_tokens, new_carried)
 
 

time: 153 us -> 67.5 us (0.44)
  Pallas kernels: 0 us -> 50.4 us
  waiting for transfers between devices: 45.9 us -> 0 us
  blocking collectives: 44.6 us -> 0 us
  matrix products: 33.3 us -> 4.59 us
  between operations: 14.3 us -> 0.77 us
  starting transfers between devices: 6.98 us -> 0 us
  local copies, waits for them, and re-layouts: 3.47 us -> 6.65 us
    pallas_call x0 -> x1, Pallas kernels: none -> 50.4 us  [experts(): pl.pallas_call(functools.partial(expert_kernel, group_size), out_shape=ja...]
    all_to_all x1 -> x0, blocking collectives: 44.6 us -> none  [per_device(): lax.all_to_all(outgoing, 'ep', split_axis=0, concat_axis=0, tiled=True)]
    dot_general x5 -> x0, matrix products: 28.6 us -> none  [the longest x1 16.3 us: per_device(): produced = jnp.dot(hidden, w_down, preferred_element_type=jnp.float32)]
    psum x1 -> x0, waiting for transfers between devices: 20 us -> none  [per_device(): lax.psum(partial_value.astype(jnp.float32).astype(jnp.bfloat16), 'tp')]
    all_to_all x1 -> x0, waiting for transfers between devices: 18.4 us -> none  [per_device(): lax.all_to_all(halves.astype(jnp.bfloat16), 'ep', split_axis=0, concat_ax...]
    reduce_scatter x1 -> x0, waiting for transfers between devices: 7.46 us -> none  [per_device(): lax.psum_scatter(produced.astype(jnp.bfloat16), 'tp', scatter_dimension=2...]
    all_to_all x1 -> x0, starting transfers between devices: 6.9 us -> none  [per_device(): lax.all_to_all(halves.astype(jnp.bfloat16), 'ep', split_axis=0, concat_ax...]
  transfers between devices with their start and end apart: 3 -> 0, of which waited for: 3 -> 0; matrix products, arithmetic and copies ran while one was open for 2% -> 0% of each run, Pallas kernels for 0% -> 0%
where the time goes in v1:
time: 67.5 us; the launch traced here: 67.2 us
  Pallas kernels  50.4 us (75%)
  local copies, waits for them, and re-layouts  6.65 us (10%)
  other arithmetic  4.84 us (7%)
  matrix products  4.59 us (7%)
  between operations  0.77 us (1%)
    pallas_call x1, Pallas kernels, experts(): pl.pallas_call(functools.partial(expert_kernel, group_size), out_shape=ja...  50.4 us
    dot_general x1, matrix products, per_device(): jnp.dot(normed, w_in, preferred_element_type=jnp.float32)  3.43 us
    unnamed x13, local copies, waits for them, and re-layouts  3 us
    slice x1, local copies, waits for them, and re-layouts, state_update(): imag_old = carried[..., half:]  1.64 us

profile of v1, /device:TPU:0, one launch (start us, length us, event | category | flops | bytes accessed | tf_op | source)
XLA Modules:
  0.0 67.2 jit_solution(8011082789098410030)
XLA Ops:
  0.6 0.7 %exp.14 = f32[48]{0:T(128)S(1)} exponential(f32[48]{0:T(128)} %param.21) | non-fusion elementwise | bytes 384 | tf_op jit(solution)/shard_map/exp | solution.py:25
  1.3 0.9 %cosine_multiply_fusion = (f32[48,64]{1,0:T(8,128)S(1)}, f32[48,64]{1,0:T(8,128)S(1)}, f32[48,64]{1,0:T(8,128)S(1)}, f32[48,64]{1,0:T(8,128)S(1)}) fusion(f32[48,64]{1,0:T(8,128)} %param.20, f32[48,64]{1,0:T(8,128)} %param.19, f32[48]{0:T(128)S(1)} %exp.14), kind=kLoop, calls=%fused_computation.35 | loop fusion | flops 58368 | bytes 73920 | tf_op jit(solution)/shard_map/mul | solution.py:27
  2.3 1.6 %fusion.23 = (f32[32,48,64]{2,1,0:T(8,128)S(1)}, f32[32,48,64]{2,1,0:T(8,128)S(1)}) fusion(f32[32,48,128]{2,1,0:T(8,128)} %param.18), kind=kLoop, calls=%fused_computation.47 | loop fusion | bytes 1572864 | tf_op jit(solution)/shard_map/slice | solution.py:42
  3.9 1.1 %fusion.4 = f32[32]{0:T(128)S(1)} fusion(bf16[32,3072]{1,0:T(8,128)(2,1)} %tokens.1), kind=kLoop, calls=%fused_computation.11 | loop fusion | flops 294880 | bytes 196736 | tf_op jit(solution)/shard_map/reduce_sum | solution.py:17
  5.0 3.4 %convolution_convert_fusion = bf16[32,768]{1,0:T(8,128)(2,1)S(1)} fusion(bf16[3072,768]{1,0:T(8,128)(2,1)} %param.26, bf16[32,3072]{1,0:T(8,128)(2,1)} %tokens.1, f32[3072]{0:T(1024)} %param.25, f32[32]{0:T(128)S(1)} %add_rsqrt_fusion), kind=kOutput, calls=%fused_computation.1 | convolution fusion | flops 151412736 | bytes 4976768 | tf_op jit(solution)/shard_map/dot_general | solution.py:451
  8.5 0.2 copy.49
  8.7 0.3 convolution_bitcast_fusion
  9.0 0.8 %fusion.22 = (f32[32,48,64]{2,0,1:T(8,128)S(1)}, f32[32,48,64]{2,0,1:T(8,128)S(1)}, f32[32,48,64]{2,0,1:T(8,128)S(1)}) fusion(f32[32,48,128]{2,0,1:T(8,128)S(1)} %convolution_bitcast_fusion, f32[48,64]{1,0:T(8,128)S(1)} %get-tuple-element.19, f32[48,64]{1,0:T(8,128)S(1)} %get-tuple-element.20, f32[32,48,64]{2,1,0:T(8,128)S(1)} %get-tuple-element.16, ...), kind=kLoop, calls=%fused_computation.46 | loop fusion | flops 1474560 | bytes 2801664 | tf_op jit(solution)/shard_map/neg | solution.py:45
  9.8 0.8 %fusion = f32[48,32,16]{1,2,0:T(8,128)S(1)} fusion(bf16[48,16,128]{2,1,0:T(8,128)(2,1)S(1)} %copy-done.1, f32[32,48,64]{2,0,1:T(8,128)S(1)} %get-tuple-element.12, f32[32,48,64]{2,0,1:T(8,128)S(1)} %get-tuple-element.14), kind=kOutput, calls=%fused_computation.2 | convolution fusion | flops 37945344 | bytes 1081344 | tf_op jit(solution)/shard_map/sgq,ghq->sgh/dot_general | solution.py:46
  10.7 0.1 copy.50
  10.8 0.7 %fusion.17.activated = bf16[32,768]{1,0:T(8,128)(2,1)} fusion(f32[32,768]{1,0:T(8,128)S(1)} %copy.50, bf16[32,768]{1,0:T(8,128)(2,1)S(1)} %convolution_convert_fusion, f32[768]{0:T(1024)S(1)} %copy-done.2), kind=kLoop, calls=%fused_computation.24 | loop fusion | flops 294912 | bytes 199680 | tf_op jit(solution)/shard_map/convert_element_type | solution.py:50
  11.5 0.1 copy.51
  11.6 0.1 eq.31
  11.7 0.1 reduce_window_sum.11
  11.8 0.2 select_reduce_fusion.1
  12.0 0.1 reduce_sum.40
  12.1 0.1 copy.52
  12.3 0.1 select_reduce_fusion
  12.4 0.6 fusion.20
  13.0 0.7 %copy.53.pack = bf16[128,32]{1,0:T(8,128)(2,1)} copy(bf16[128,32]{0,1:T(8,128)(2,1)S(1)} %get-tuple-element.11) | data formatting | bytes 16384 | tf_op jit(solution)/shard_map/convert_element_type | solution.py:466
  13.7 50.4 %shard_map.176 = bf16[32,1536]{1,0:T(8,128)(2,1)} custom-call(bf16[32,3072]{1,0:T(8,128)(2,1)} %tokens.1, bf16[32,768]{1,0:T(8,128)(2,1)} %fusion.17.activated, f32[1,3072]{1,0:T(1,128)} %bitcast.20, bf16[128,32]{1,0:T(8,128)(2,1)} %copy.53.pack, bf16[32,128]{1,0:T(8,128)(2,1)} %get-tuple-element.22.weight_high, ...), custom_call_target="tpu_custom_call" | custom-call | tf_op jit(solution)/shard_map/pallas_call | solution.py:384
  64.1 0.3 pad_maximum_fusion
  64.4 1.3 %copy.54 = f32[32,48,128]{2,1,0:T(8,128)} copy(f32[32,48,128]{2,0,1:T(8,128)S(1)} %pad_maximum_fusion) | data formatting | bytes 1572864
  65.7 1.5 %copy.64 = bf16[32,1536]{1,0:T(8,128)(2,1)} copy(bf16[32,1536]{1,0:T(8,128)(2,1)} %shard_map.176) | data formatting | bytes 196608
  (15 shorter events, 0.2 us)
Async XLA Ops:
  0.6 8.0 %copy-start = (bf16[48,128,16]{1,2,0:T(8,128)(2,1)S(1)}, bf16[48,128,16]{1,2,0:T(8,128)(2,1)}, u32[]{:S(2)}) copy-start(bf16[48,128,16]{1,2,0:T(8,128)(2,1)} %param.22) | copy-start | bytes 589828
  8.6 1.2 %copy-start.1 = (bf16[48,16,128]{2,1,0:T(8,128)(2,1)S(1)}, bf16[48,16,128]{2,1,0:T(8,128)(2,1)}, u32[]{:S(2)}) copy-start(bf16[48,16,128]{2,1,0:T(8,128)(2,1)} %param.23) | copy-start | bytes 589828
  8.6 2.1 %copy-start.2 = (f32[768]{0:T(1024)S(1)}, f32[768]{0:T(1024)}, u32[]{:S(2)}) copy-start(f32[768]{0:T(1024)} %param.24) | copy-start | bytes 9220
  8.7 2.8 %copy-start.3 = (s32[32,2]{0,1:T(2,128)S(1)}, s32[32,2]{0,1:T(2,128)}, u32[]{:S(2)}) copy-start(s32[32,2]{0,1:T(2,128)} %param.29) | copy-start | bytes 772
  8.7 3.6 %copy-start.4 = (f32[32,2]{0,1:T(2,128)S(1)}, f32[32,2]{0,1:T(2,128)}, u32[]{:S(2)}) copy-start(f32[32,2]{0,1:T(2,128)} %param.30) | copy-start | bytes 772
